TPU v7x, 256 devices: a whole 4x4x8 slice. The times are simulated.
256 devices in a mesh: sp: 32 (over z, y), tp: 8 (over x, core).
Axes of the slice: x: 4, y: 4, z: 8, core: 2. Of those that a mesh axis runs over, the one named last changes fastest.
Arguments:
- tokens: bfloat16 [32768, 2048], P('sp'), may hold values from -6 to 6
- in_gain: float32 [2048], replicated, may hold values from 0.1 to 1.9
- w_query: bfloat16 [2048, 1024], P(None, 'tp'), may hold values from -0.125 to 0.125
- w_forget: bfloat16 [2048, 1024], P(None, 'tp'), may hold values from -0.125 to 0.125
- w_input: bfloat16 [2048, 1024], P(None, 'tp'), may hold values from -0.125 to 0.125
- w_outgate: bfloat16 [2048, 1024], P(None, 'tp'), may hold values from -0.125 to 0.125
- w_conv_h: bfloat16 [2048, 1024], P(None, 'tp'), may hold values from -0.125 to 0.125
- w_conv_b: bfloat16 [2048, 1024], P(None, 'tp'), may hold values from -0.125 to 0.125
- w_conv_c: bfloat16 [2048, 1024], P(None, 'tp'), may hold values from -0.125 to 0.125
- forget_floor: float32 [1024], P('tp'), may hold values from 0.84 to 1
- forget_leak: float32 [32768, 1024], P('sp', 'tp'), may hold values from -1 to 0
- state_gain: float32 [128], replicated, may hold values from 0.1 to 1.9
- conv_taps: bfloat16 [3, 1024], P(None, 'tp'), may hold values from -3.5 to 3.5
- group_gain: float32 [128], replicated, may hold values from 0.1 to 1.9
- out_state: bfloat16 [1024, 2048], P('tp'), may hold values from -0.1875 to 0.1875
- out_conv: bfloat16 [1024, 2048], P('tp'), may hold values from -0.1875 to 0.1875
Outputs:
- mixed_out: bfloat16 [32768, 2048], P('sp', 'tp')
All inputs are finite; a program needn't handle non-finite values.
Results may differ from a plain program's by a relative error of at most 0.015.
Values may be sent and summed in bfloat16 or wider, within the bound.
No kernel may reach another device: no remote copies, remote signals or barrier semaphores. Data moves between devices by JAX's collectives and lax.ppermute only.
A program may use at most 128 MiB of HBM per device.

v0:
```python
import jax
import jax.numpy as jnp
from jax import lax
from jax.sharding import Mesh
from jax.sharding import PartitionSpec as P

GROUP_FEATURES = 128
BLOCK = 64
TAPS = 3
SP = ("sp_0", "sp_1")
norm_eps = 1e-06


def from_behind(array, axis, by):
    count = lax.axis_size(axis)
    pairs = [(i, i + by) for i in range(count) if 0 <= i + by < count]
    return lax.ppermute(array, axis, pairs)


def neutral_like(array, identity):
    return jax.tree.map(
        lambda part, zero: jnp.zeros_like(part) + jnp.asarray(zero, part.dtype), array, identity
    )


def collected_together(array, axis):
    leaves = jax.tree.leaves(array)
    turns = sorted(range(len(leaves)), key=lambda k: -leaves[k].size)
    width = (1, *leaves[turns[0]].shape)[-1]
    lines = [
        jnp.pad(leaves[k].reshape(-1), (0, -leaves[k].size % width)).reshape(-1, width)
        for k in turns
    ]
    both, at, found = (lax.all_gather(jnp.concatenate(lines), axis), 0, {})
    for k, line in zip(turns, lines):
        section = both[:, at : at + len(line)].reshape(len(both), -1)
        found[k] = section[:, : leaves[k].size].reshape(-1, *leaves[k].shape)
        at += len(line)
    numbers = iter(range(len(leaves)))
    return jax.tree.map(lambda _: found[next(numbers)], array)


def carried_in(array, axes, combine, identity):
    before = start = neutral_like(array, identity)
    subtotal = array
    for axis in reversed(axes):
        count, index = (lax.axis_size(axis), lax.axis_index(axis))
        pieces = collected_together(
            jax.tree.map(
                lambda part, kind: part.astype(kind), subtotal, (jnp.bfloat16, jnp.bfloat16)
            ),
            axis,
        )
        inside, subtotal = (start, start)
        for k in range(count):
            passed = k < index
            subtotal = combine(
                subtotal, jax.tree.map(lambda part, own: part[k].astype(own.dtype), pieces, array)
            )
            inside = jax.tree.map(lambda new, old: jnp.where(passed, new, old), subtotal, inside)
        before = combine(inside, before)
    return before


def rms_rows(values, gain):
    scale = lax.rsqrt(jnp.mean(values * values, axis=-1, keepdims=True) + norm_eps)
    return values * scale * gain


def state_block(carry, inputs):
    carry_state, offset = carry
    query_blk, key_blk, value_blk, logf_blk = inputs
    cum_log = jnp.cumsum(logf_blk, axis=1)
    carried = jnp.einsum("hcd,hde->hce", query_blk * jnp.exp(cum_log), carry_state)
    length = logf_blk.shape[1]
    causal = (jnp.arange(length)[:, None] >= jnp.arange(length)[None, :])[None, :, :, None]
    diff_log = cum_log[:, :, None, :] - cum_log[:, None, :, :]
    decay_all = jnp.exp(jnp.where(causal, diff_log, -jnp.inf))
    scores = jnp.einsum("hid,hjd,hijd->hij", query_blk, key_blk, decay_all)
    result = carried + jnp.einsum("hij,hje->hie", scores, value_blk)
    last_log = cum_log[:, -1, :]
    fresh = jnp.einsum("hcd,hce->hde", key_blk * jnp.exp(last_log[:, None, :] - cum_log), value_blk)
    new_state = jnp.exp(last_log)[:, :, None] * carry_state + fresh
    return ((new_state, offset + last_log), (result, offset[:, None, :] + cum_log))


def join_states(earlier, later):
    earlier_log, earlier_state = earlier
    later_log, later_state = later
    return (earlier_log + later_log, jnp.exp(later_log)[:, :, None] * earlier_state + later_state)


def body(
    tokens,
    in_gain,
    w_query,
    w_forget,
    w_input,
    w_outgate,
    w_conv_h,
    w_conv_b,
    w_conv_c,
    forget_floor,
    forget_leak,
    state_gain,
    conv_taps,
    group_gain,
    out_state,
    out_conv,
):
    count = tokens.shape[0]
    heads = w_query.shape[1] // GROUP_FEATURES
    channels = w_conv_h.shape[1]
    normed = rms_rows(tokens.astype(jnp.float32), in_gain).astype(jnp.bfloat16)

    def project(weight):
        return jnp.dot(normed, weight, preferred_element_type=jnp.float32).astype(jnp.bfloat16)

    proj_query = project(w_query)
    proj_forget = project(w_forget)
    proj_input = project(w_input)
    proj_outgate = project(w_outgate)
    proj_h = project(w_conv_h)
    proj_b = project(w_conv_b)
    proj_c = project(w_conv_c)
    conv_in = (proj_c.astype(jnp.float32) * proj_h.astype(jnp.float32)).astype(jnp.bfloat16)
    rim_rows = from_behind(conv_in[count - (TAPS - 1) :], SP, 1)
    gate_logit = proj_forget.astype(jnp.float32)
    log_forget = (
        jnp.logaddexp(
            jnp.log(forget_floor), jnp.log1p(-forget_floor) + jax.nn.log_sigmoid(gate_logit)
        )
        + forget_leak
    )
    key_gate = (1.0 - forget_floor) * jax.nn.sigmoid(-gate_logit)
    query_act = jax.nn.silu(proj_query.astype(jnp.float32))
    value_f = proj_input.astype(jnp.float32)
    nblk = count // BLOCK

    def to_blocks(arr):
        return arr.reshape(nblk, BLOCK, heads, GROUP_FEATURES).transpose(0, 2, 1, 3)

    def from_blocks(arr):
        return arr.transpose(0, 2, 1, 3).reshape(count, heads, GROUP_FEATURES)

    start_state = jnp.zeros((heads, GROUP_FEATURES, GROUP_FEATURES), jnp.float32)
    start_log = jnp.zeros((heads, GROUP_FEATURES), jnp.float32)
    (local_state, total_log), (local_read, cum_blocks) = lax.scan(
        state_block,
        (start_state, start_log),
        (to_blocks(query_act), to_blocks(key_gate), to_blocks(value_f), to_blocks(log_forget)),
    )
    _, incoming = carried_in((total_log, local_state), SP, join_states, (start_log, start_state))
    cum_device = from_blocks(cum_blocks)
    query_heads = query_act.reshape(count, heads, GROUP_FEATURES)
    cross = jnp.einsum("thd,hde->the", query_heads * jnp.exp(cum_device), incoming)
    state_read = from_blocks(local_read) + cross
    out_gate = jax.nn.silu(proj_outgate.astype(jnp.float32)).reshape(count, heads, GROUP_FEATURES)
    state_res = (
        (rms_rows(state_read, state_gain) * out_gate)
        .reshape(count, heads * GROUP_FEATURES)
        .astype(jnp.bfloat16)
    )
    padded = jnp.concatenate([rim_rows, conv_in], axis=0).astype(jnp.float32)
    taps_f = conv_taps.astype(jnp.float32)
    conv_sum = jnp.zeros((count, channels), jnp.float32)
    for offset in range(TAPS):
        conv_sum = conv_sum + taps_f[offset][None, :] * padded[offset : offset + count]
    gated = (proj_b.astype(jnp.float32) * conv_sum).reshape(
        count, channels // GROUP_FEATURES, GROUP_FEATURES
    )
    conv_res = rms_rows(gated, group_gain).reshape(count, channels).astype(jnp.bfloat16)
    mixed_here = jnp.concatenate([state_res, conv_res], axis=1)
    weight_rows = jnp.concatenate([out_state, out_conv], axis=0)
    columns = lax.all_to_all(weight_rows, "tp", split_axis=1, concat_axis=0, tiled=True)
    summed = jnp.dot(
        lax.all_gather(mixed_here, "tp", axis=1, tiled=True),
        columns,
        preferred_element_type=jnp.float32,
    )
    return summed.astype(jnp.bfloat16)


def solution(mesh):
    split = Mesh(mesh.devices.reshape(8, 4, mesh.shape["tp"]), ("sp_0", "sp_1", "tp"))
    placed = (
        P(SP, None),
        P(),
        P(None, "tp"),
        P(None, "tp"),
        P(None, "tp"),
        P(None, "tp"),
        P(None, "tp"),
        P(None, "tp"),
        P(None, "tp"),
        P("tp"),
        P(SP, "tp"),
        P(),
        P(None, "tp"),
        P(),
        P("tp", None),
        P("tp", None),
    )
    return jax.shard_map(body, mesh=split, in_specs=placed, out_specs=P(SP, "tp"), check_vma=False)
```

profile of v0, /device:TPU:1, one launch (start us, length us, event | category | flops | bytes accessed | tf_op | source)
XLA Modules:
  0.0 187.0 jit_solution(12285283551542501446)
XLA Ops:
  6.5 3.2 %fusion.30 = f32[1024]{0:T(1024)S(1)} fusion(bf16[1024,2048]{1,0:T(8,128)(2,1)} %param.18), kind=kLoop, calls=%fused_computation.44 | loop fusion | flops 6290432 | bytes 4198400 | tf_op jit(solution)/shard_map/reduce_sum | solution.py:66
  10.1 1.0 fusion.32
  11.1 1.2 fusion.37
  12.5 1.3 fusion.36
  13.8 4.0 %collective-permute-start = (bf16[2,128]{1,0:T(2,128)(2,1)S(1)}, bf16[2,128]{1,0:T(2,128)(2,1)S(1)}, u32[]{:S(2)}, u32[]{:S(2)}) collective-permute-start(bf16[2,128]{1,0:T(2,128)(2,1)S(1)} %slice.193), channel_id=1, source_target_pairs={{0,8},{8,16},{16,24},{24,32},{32,40},{40,48},{48,56},{56,64},{64,7... | collective-permute-start | bytes 1544 | tf_op jit(solution)/shard_map/ppermute | solution.py:17
  18.0 3.6 %divide_multiply_fusion = f32[1024,128]{1,0:T(8,128)S(1)} fusion(bf16[1024,2048]{1,0:T(8,128)(2,1)} %copy-done.1, bf16[2048,128]{1,0:T(8,128)(2,1)S(1)} %copy-done.13), kind=kOutput, calls=%fused_computation.83 | convolution fusion | flops 537657344 | bytes 5242880 | tf_op jit(solution)/shard_map/dot_general | solution.py:117
  21.6 1.2 convolution_convert_fusion.6
  22.9 1.8 divide_multiply_fusion.1
  24.6 58.7 %while.17 = (s32[]{:T(128)}, f32[1,128,128]{2,1,0:T(8,128)S(1)}, f32[1,128]{1,0:T(1,128)S(1)}, f32[16,1,64,128]{3,2,1,0:T(8,128)}, f32[16,1,64,128]{3,2,1,0:T(8,...) while((s32[]{:T(128)}, f32[1,128,128]{2,1,0:T(8,128)S(1)}, ...), condition=%wide.region_3.4_spmd.clone, body=%wide.region_1.3_spmd.clone.sunk | while | flops 8487171 | bytes 5119637 | solution.py:148
  25.4 1.7 fusion.189
  27.3 0.8 fusion.190
  29.1 1.7 fusion.189
  30.9 0.8 fusion.190
  32.8 1.7 fusion.189
  34.6 0.8 fusion.190
  36.4 1.7 fusion.189
  38.3 0.8 fusion.190
  40.1 1.7 fusion.189
  41.9 0.8 fusion.190
  43.8 1.7 fusion.189
  45.6 0.8 fusion.190
  47.4 1.7 fusion.189
  49.3 0.8 fusion.190
  51.1 1.7 fusion.189
  52.9 0.8 fusion.190
  54.8 1.7 fusion.189
  58.4 1.7 fusion.189
  60.3 0.8 fusion.190
  62.1 1.7 fusion.189
  63.9 0.8 fusion.190
  65.8 1.7 fusion.189
  67.6 0.8 fusion.190
  69.4 1.7 fusion.189
  73.1 1.7 fusion.189
  75.0 0.8 fusion.190
  76.8 1.7 fusion.189
  78.6 0.8 fusion.190
  80.4 1.7 fusion.189
  82.3 0.8 fusion.190
  83.4 9.5 %all-gather.2 = bf16[4,129,128]{2,1,0:T(8,128)(2,1)S(1)} all-gather(bf16[1,129,128]{2,1,0:T(8,128)(2,1)S(1)} %maximum_bitcast_fusion), channel_id=2, replica_groups=mesh['sp_0'=8,'sp_1'=4,'tp'=8] {'sp_1'}, dimensions={0}, use_global_device_ids=true | all-gather | bytes 165120 | tf_op jit(solution)/shard_map/all_gather | solution.py:34
  93.1 22.4 %all-gather.3 = bf16[8,129,128]{2,1,0:T(8,128)(2,1)S(1)} all-gather(bf16[1,129,128]{2,1,0:T(8,128)(2,1)S(1)} %maximum_bitcast_fusion.1), channel_id=3, replica_groups=mesh['sp_0'=8,'sp_1'=4,'tp'=8] {'sp_0'}, dimensions={0}, use_global_device_ids=true | all-gather | bytes 297216 | tf_op jit(solution)/shard_map/all_gather | solution.py:34
  115.6 1.7 multiply_reduce_fusion.1
  117.4 3.6 %fusion.48 = bf16[1024,128]{1,0:T(8,128)(2,1)S(1)} fusion(bf16[1024,2048]{1,0:T(8,128)(2,1)} %copy-done.1, bf16[2048,128]{1,0:T(8,128)(2,1)S(1)} %copy-done.16, f32[1024,1,128]{2,0,1:T(8,128)S(1)} %get-tuple-element.181, f32[128]{0:T(128)S(1)} %copy-done.18, f32[1024]{0:T(1024)S(1)} %add_rsqrt_fusion.1), kind=kOutput, calls=%fused_computation.81 | convolution fusion | flops 538181632 | bytes 5509632 | tf_op jit(solution)/shard_map/dot_general | solution.py:117
  121.2 1.3 multiply_reduce_fusion
  122.8 0.9 pad_maximum_fusion.1
  124.3 34.8 %all_to_all.19 = bf16[256,8,256]{0,2,1:T(8,128)(2,1)S(1)} all-to-all(bf16[256,8,256]{0,2,1:T(8,128)(2,1)S(1)} %bitcast.205), channel_id=1, replica_groups=mesh['sp_0'=8,'sp_1'=4,'tp'=8] {'tp'}, dimensions={1} | all-to-all | bytes 2097152 | tf_op jit(solution)/shard_map/all_to_all | solution.py:175
  159.6 16.3 %all-gather.6.cloned.1.call-done = bf16[1024,2048]{1,0:T(8,128)(2,1)} async-done(((bf16[1024,256]{1,0:T(8,128)(2,1)}), bf16[1024,2048]{1,0:T(8,128)(2,1)}) %all-gather.6.cloned.1.call-update) | async-done | bytes 4194320 | tf_op jit(solution)/shard_map/all_gather | solution.py:177
  176.0 4.2 %convolution_convert_fusion = bf16[1024,256]{1,0:T(8,128)(2,1)} fusion(bf16[1024,2048]{1,0:T(8,128)(2,1)} %all-gather.6.cloned.1.call-done, bf16[2048,256]{1,0:T(8,128)(2,1)S(1)} %bitcast.209), kind=kOutput, calls=%fused_computation.48 | convolution fusion | flops 1074003968 | bytes 5767168 | tf_op jit(solution)/shard_map/dot_general | solution.py:176
  (245 shorter events, 21.6 us)
Async XLA Ops:
  6.5 16.3 %copy-start = (bf16[2048,128]{1,0:T(8,128)(2,1)S(1)}, bf16[2048,128]{1,0:T(8,128)(2,1)}, u32[]{:S(2)}) copy-start(bf16[2048,128]{1,0:T(8,128)(2,1)} %param.21) | copy-start | bytes 1572868
  6.5 3.2 %copy-start.9 = (f32[2048]{0:T(1024)S(1)}, f32[2048]{0:T(1024)}, u32[]{:S(2)}) copy-start(f32[2048]{0:T(1024)} %param.19) | copy-start | bytes 24580
  6.5 169.4 %all-gather.6.cloned.1.call-start = ((), (), s32[]{:S(2)}) async-start(), calls=%async_computation.1 | async-start | bytes 4718592 | tf_op jit(solution)/shard_map/all_gather | solution.py:177
  6.5 3.5 %copy-start.4 = (bf16[1024,2048]{1,0:T(8,128)(2,1)S(1)}, bf16[1024,2048]{1,0:T(8,128)(2,1)}, u32[]{:S(2)}) copy-start(bf16[1024,2048]{1,0:T(8,128)(2,1)} %param.18) | copy-start | bytes 12582916
  10.1 1.0 copy-start.5
  11.1 2.7 %copy-start.1 = (bf16[1024,2048]{1,0:T(8,128)(2,1)}, bf16[1024,2048]{1,0:T(8,128)(2,1)S(1)}, u32[]{:S(2)}) copy-start(bf16[1024,2048]{1,0:T(8,128)(2,1)S(1)} %fusion.32) | copy-start | bytes 12582916
  11.1 1.4 copy-start.6
  12.5 5.4 %copy-start.11 = (f32[128]{0:T(128)S(1)}, f32[128]{0:T(128)}, u32[]{:S(2)}) copy-start(f32[128]{0:T(128)} %param.27) | copy-start | bytes 1540
  12.5 5.4 %copy-start.13 = (bf16[2048,128]{1,0:T(8,128)(2,1)S(1)}, bf16[2048,128]{1,0:T(8,128)(2,1)}, u32[]{:S(2)}) copy-start(bf16[2048,128]{1,0:T(8,128)(2,1)} %param.20) | copy-start | bytes 1572868
  13.8 107.2 %collective-permute-start = (bf16[2,128]{1,0:T(2,128)(2,1)S(1)}, bf16[2,128]{1,0:T(2,128)(2,1)S(1)}, u32[]{:S(2)}, u32[]{:S(2)}) collective-permute-start(bf16[2,128]{1,0:T(2,128)(2,1)S(1)} %slice.193), channel_id=1, source_target_pairs={{0,8},{8,16},{16,24},{24,32},{32,40},{40,48},{48,56},{56,64},{64,7... | collective-permute-start | bytes 1544 | tf_op jit(solution)/shard_map/ppermute | solution.py:17
  17.9 3.6 %copy-start.2 = (bf16[1024,2048]{1,0:T(8,128)(2,1)S(1)}, bf16[1024,2048]{1,0:T(8,128)(2,1)}, u32[]{:S(2)}) copy-start(bf16[1024,2048]{1,0:T(8,128)(2,1)} %copy-done.1) | copy-start | bytes 12582916
  18.0 3.6 %copy-start.14 = (bf16[2048,128]{1,0:T(8,128)(2,1)S(1)}, bf16[2048,128]{1,0:T(8,128)(2,1)}, u32[]{:S(2)}) copy-start(bf16[2048,128]{1,0:T(8,128)(2,1)} %param.22) | copy-start | bytes 1572868
  21.6 1.3 copy-start.15
  83.3 34.0 %copy-start.10 = (bf16[3,128]{1,0:T(4,128)(2,1)S(1)}, bf16[3,128]{1,0:T(4,128)(2,1)}, u32[]{:S(2)}) copy-start(bf16[3,128]{1,0:T(4,128)(2,1)} %param.30) | copy-start | bytes 2308
  83.4 34.1 %copy-start.16 = (bf16[2048,128]{1,0:T(8,128)(2,1)S(1)}, bf16[2048,128]{1,0:T(8,128)(2,1)}, u32[]{:S(2)}) copy-start(bf16[2048,128]{1,0:T(8,128)(2,1)} %param.23) | copy-start | bytes 1572868
  83.4 34.1 %copy-start.18 = (f32[128]{0:T(128)S(1)}, f32[128]{0:T(128)}, u32[]{:S(2)}) copy-start(f32[128]{0:T(128)} %param.29) | copy-start | bytes 1540
  117.4 3.7 %copy-start.3 = (bf16[1024,2048]{1,0:T(8,128)(2,1)S(1)}, bf16[1024,2048]{1,0:T(8,128)(2,1)}, u32[]{:S(2)}) copy-start(bf16[1024,2048]{1,0:T(8,128)(2,1)} %copy-done.1) | copy-start | bytes 12582916
  117.4 3.7 %copy-start.17 = (bf16[2048,128]{1,0:T(8,128)(2,1)S(1)}, bf16[2048,128]{1,0:T(8,128)(2,1)}, u32[]{:S(2)}) copy-start(bf16[2048,128]{1,0:T(8,128)(2,1)} %param.25) | copy-start | bytes 1572868
  121.2 1.4 copy-start.12
  121.2 2.5 %copy-start.7 = (bf16[128,2048]{1,0:T(8,128)(2,1)S(1)}, bf16[128,2048]{1,0:T(8,128)(2,1)}, u32[]{:S(2)}) copy-start(bf16[128,2048]{1,0:T(8,128)(2,1)} %param.32) | copy-start | bytes 1572868
  121.2 2.7 %copy-start.8 = (bf16[128,2048]{1,0:T(8,128)(2,1)S(1)}, bf16[128,2048]{1,0:T(8,128)(2,1)}, u32[]{:S(2)}) copy-start(bf16[128,2048]{1,0:T(8,128)(2,1)} %param.33) | copy-start | bytes 1572868
Sparse Core Ops, SparseCore 0:
  123.8 52.1 all-gather.5
where the time goes:
time: 187 us
  blocking collectives  66.6 us (36%)
  other arithmetic  44.8 us (24%)
  matrix products  38.1 us (20%)
  waiting for transfers between devices  16.4 us (9%)
  between operations  13.9 us (7%)
  starting transfers between devices  4.02 us (2%)
  local copies, waits for them, and re-layouts  2.2 us (1%)
    all_to_all x1, blocking collectives, body(): lax.all_to_all(weight_rows, 'tp', split_axis=1, concat_axis=0, tiled=True)  34.8 us
    all_gather x2, blocking collectives, collected_together(): both, at, found = (lax.all_gather(jnp.concatenate(lines), axis), 0, {})  31.9 us
    dot_general x16, other arithmetic, state_block(): scores = jnp.einsum('hid,hjd,hijd->hij', query_blk, key_blk, decay_all)  27.3 us
    all_gather x1, waiting for transfers between devices, body(): lax.all_gather(mixed_here, 'tp', axis=1, tiled=True)  16.3 us
    dot_general x7, matrix products, project(): jnp.dot(normed, weight, preferred_element_type=jnp.float32)  14 us
    dot_general x16, matrix products, state_block(): result = carried + jnp.einsum('hij,hje->hie', scores, value_blk)  12.7 us
    exp x16, other arithmetic, state_block(): decay_all = jnp.exp(jnp.where(causal, diff_log, -jnp.inf))  9.79 us
    dot_general x1, matrix products, body(): jnp.dot(lax.all_gather(mixed_here, 'tp', axis=1, tiled=True), columns, pr...  4.23 us
  transfers between devices with their start and end apart: 2, of which 1 were waited for; matrix products, arithmetic and copies ran while one was open for 38% of the time, Pallas kernels for 0%

commit v1 on v0

--- a/solution.py
+++ b/solution.py
@@ -173,11 +173,10 @@
     mixed_here = jnp.concatenate([state_res, conv_res], axis=1)
     weight_rows = jnp.concatenate([out_state, out_conv], axis=0)
     columns = lax.all_to_all(weight_rows, "tp", split_axis=1, concat_axis=0, tiled=True)
-    summed = jnp.dot(
-        lax.all_gather(mixed_here, "tp", axis=1, tiled=True),
-        columns,
-        preferred_element_type=jnp.float32,
-    )
+    pools_obtain = lambda sheet: jnp.concatenate(
+        lax.all_to_all(jnp.stack([sheet for _ in range(lax.axis_size("tp"))]), "tp", 0, 0), axis=1
+    )
+    summed = jnp.dot(pools_obtain(mixed_here), columns, preferred_element_type=jnp.float32)
     return summed.astype(jnp.bfloat16)
 
 

time: 187 us -> 228 us (1.22); the launches traced: 187 us -> 225 us
  blocking collectives: 66.6 us -> 94.3 us
  matrix products: 38.1 us -> 60.7 us
  waiting for transfers between devices: 16.4 us -> 0.01 us
  between operations: 13.9 us -> 0.41 us
  local copies, waits for them, and re-layouts: 2.2 us -> 15.3 us
  starting transfers between devices: 4.02 us -> 9.27 us
    all_to_all x1, blocking collectives: 34.8 us -> 62.6 us  [body(): lax.all_to_all(jnp.stack([sheet for _ in range(lax.axis_size('tp'))]), 't...]
    all_gather x1 -> x0, waiting for transfers between devices: 16.3 us -> none  [body(): lax.all_gather(mixed_here, 'tp', axis=1, tiled=True)]
    squeeze x16, local copies, waits for them, and re-layouts: 0.14 us -> 12.2 us  [body(): lax.scan(state_block, (start_state, start_log), (to_blocks(query_act), to...]
    dot_general x16, matrix products: 3.26 us -> 14.8 us  [state_block(): jnp.einsum('hcd,hce->hde', key_blk * jnp.exp(last_log[:, None, :] - cum_l...]
    dot_general x16, matrix products: 12.7 us -> 24.2 us  [state_block(): result = carried + jnp.einsum('hij,hje->hie', scores, value_blk)]
    all_to_all x0 -> x1, starting transfers between devices: none -> 5.25 us  [body(): lax.all_to_all(weight_rows, 'tp', split_axis=1, concat_axis=0, tiled=True)]
  transfers between devices with their start and end apart: 2 -> 2, of which waited for: 1 -> 0; matrix products, arithmetic and copies ran while one was open for 38% -> 49% of each run, Pallas kernels for 0% -> 0%
where the time goes in v1:
time: 228 us; the launch traced here: 225 us
  blocking collectives  94.3 us (41%)
  matrix products  60.7 us (27%)
  other arithmetic  44.1 us (19%)
  local copies, waits for them, and re-layouts  15.3 us (7%)
  starting transfers between devices  9.27 us (4%)
    all_to_all x1, blocking collectives, body(): lax.all_to_all(jnp.stack([sheet for _ in range(lax.axis_size('tp'))]), 't...  62.6 us
    all_gather x2, blocking collectives, collected_together(): both, at, found = (lax.all_gather(jnp.concatenate(lines), axis), 0, {})  31.7 us
    dot_general x16, other arithmetic, state_block(): scores = jnp.einsum('hid,hjd,hijd->hij', query_blk, key_blk, decay_all)  27.4 us
    dot_general x16, matrix products, state_block(): result = carried + jnp.einsum('hij,hje->hie', scores, value_blk)  24.2 us
    dot_general x7, matrix products, project(): jnp.dot(normed, weight, preferred_element_type=jnp.float32)  15.8 us
    dot_general x16, matrix products, state_block(): jnp.einsum('hcd,hce->hde', key_blk * jnp.exp(last_log[:, None, :] - cum_l...  14.8 us
    squeeze x16, local copies, waits for them, and re-layouts, body(): lax.scan(state_block, (start_state, start_log), (to_blocks(query_act), to...  12.2 us
    exp x16, other arithmetic, state_block(): decay_all = jnp.exp(jnp.where(causal, diff_log, -jnp.inf))  9.79 us
  transfers between devices with their start and end apart: 2, of which 0 were waited for; matrix products, arithmetic and copies ran while one was open for 49% of the time, Pallas kernels for 0%

profile of v1, /device:TPU:1, one launch (start us, length us, event | category | flops | bytes accessed | tf_op | source)
XLA Modules:
  0.0 224.9 jit_solution(2378140934067303725)
XLA Ops:
  0.0 3.2 %fusion.30 = f32[1024]{0:T(1024)S(1)} fusion(bf16[1024,2048]{1,0:T(8,128)(2,1)} %param.18), kind=kLoop, calls=%fused_computation.44 | loop fusion | flops 6290432 | bytes 4198400 | tf_op jit(solution)/shard_map/reduce_sum | solution.py:66
  6.0 1.3 fusion.44
  7.3 4.0 %collective-permute-start = (bf16[2,128]{1,0:T(2,128)(2,1)S(1)}, bf16[2,128]{1,0:T(2,128)(2,1)S(1)}, u32[]{:S(2)}, u32[]{:S(2)}) collective-permute-start(bf16[2,128]{1,0:T(2,128)(2,1)S(1)} %slice.193), channel_id=1, source_target_pairs={{0,8},{8,16},{16,24},{24,32},{32,40},{40,48},{48,56},{56,64},{64,7... | collective-permute-start | bytes 1544 | tf_op jit(solution)/shard_map/ppermute | solution.py:17
  12.0 1.3 copy.57
  13.3 5.2 %all-to-all-start.1 = ((bf16[256,8,256]{2,0,1:T(8,128)(2,1)}), bf16[256,8,256]{2,0,1:T(8,128)(2,1)S(1)}, u32[]{:S(2)}, u32[]{:S(2)}) async-start(bf16[256,8,256]{2,0,1:T(8,128)(2,1)} %copy.57), calls=%async_computation.1 | async-start | bytes 2097152 | tf_op jit(solution)/shard_map/all_to_all | solution.py:175
  18.6 3.7 %divide_multiply_fusion = f32[1024,128]{1,0:T(8,128)S(1)} fusion(bf16[1024,2048]{1,0:T(8,128)(2,1)} %copy-done.1, bf16[2048,128]{1,0:T(8,128)(2,1)} %param.20), kind=kOutput, calls=%fused_computation.87 | convolution fusion | flops 537657344 | bytes 5242880 | tf_op jit(solution)/shard_map/dot_general | solution.py:117
  22.3 2.0 convolution_convert_fusion.5
  24.3 2.6 %divide_multiply_fusion.1 = (f32[1024,128]{1,0:T(8,128)S(1)}, f32[1024,128]{1,0:T(8,128)}) fusion(f32[128]{0:T(128)S(1)} %get-tuple-element.166, f32[1024,128]{1,0:T(8,128)S(1)} %copy-done.14, f32[128]{0:T(128)S(1)} %get-tuple-element.168, f32[128]{0:T(128)S(1)} %get-tuple-element.167, bf16[1024,2048]{1,0:T(8,128)(2,1)S(1)} %copy-done.2, ...), kind=kOutput, calls=%fused_computation.88 | convolution fusion | flops 539885568 | bytes 6292992 | tf_op jit(solution)/shard_map/dot_general | solution.py:117
  26.9 93.7 %while.17 = (s32[]{:T(128)}, f32[1,128,128]{2,1,0:T(8,128)S(1)}, f32[1,128]{1,0:T(1,128)S(1)}, f32[16,1,64,128]{3,2,1,0:T(8,128)}, f32[16,1,64,128]{3,2,1,0:T(8,...) while((s32[]{:T(128)}, f32[1,128,128]{2,1,0:T(8,128)S(1)}, ...), condition=%wide.region_3.4_spmd.clone, body=%wide.region_1.3_spmd.clone.sunk | while | flops 8487171 | bytes 5111445 | solution.py:148
  28.4 1.7 fusion.196
  30.3 1.5 fusion.197
  34.3 1.7 fusion.196
  36.1 1.5 fusion.197
  40.1 1.7 fusion.196
  42.0 1.5 fusion.197
  46.0 1.7 fusion.196
  47.8 1.5 fusion.197
  51.8 1.7 fusion.196
  53.7 1.5 fusion.197
  57.7 1.7 fusion.196
  59.6 1.5 fusion.197
  63.6 1.7 fusion.196
  65.4 1.5 fusion.197
  69.4 1.7 fusion.196
  71.3 1.5 fusion.197
  75.3 1.7 fusion.196
  77.1 1.5 fusion.197
  81.1 1.7 fusion.196
  83.0 1.5 fusion.197
  87.0 1.7 fusion.196
  88.8 1.5 fusion.197
  92.9 1.7 fusion.196
  94.7 1.5 fusion.197
  98.7 1.7 fusion.196
  100.6 1.5 fusion.197
  104.6 1.7 fusion.196
  106.4 1.5 fusion.197
  110.4 1.7 fusion.196
  112.3 1.5 fusion.197
  116.3 1.7 fusion.196
  118.1 1.5 fusion.197
  120.7 9.4 %all-gather.2 = bf16[4,129,128]{2,1,0:T(8,128)(2,1)S(1)} all-gather(bf16[1,129,128]{2,1,0:T(8,128)(2,1)S(1)} %maximum_bitcast_fusion), channel_id=2, replica_groups=mesh['sp_0'=8,'sp_1'=4,'tp'=8] {'sp_1'}, dimensions={0}, use_global_device_ids=true | all-gather | bytes 165120 | tf_op jit(solution)/shard_map/all_gather | solution.py:34
  130.2 22.3 %all-gather.3 = bf16[8,129,128]{2,1,0:T(8,128)(2,1)S(1)} all-gather(bf16[1,129,128]{2,1,0:T(8,128)(2,1)S(1)} %maximum_bitcast_fusion.1), channel_id=3, replica_groups=mesh['sp_0'=8,'sp_1'=4,'tp'=8] {'sp_0'}, dimensions={0}, use_global_device_ids=true | all-gather | bytes 297216 | tf_op jit(solution)/shard_map/all_gather | solution.py:34
  152.7 1.7 multiply_reduce_fusion.1
  154.5 3.7 %fusion.57 = bf16[1024,128]{1,0:T(8,128)(2,1)S(1)} fusion(bf16[1024,2048]{1,0:T(8,128)(2,1)} %copy-done.1, bf16[2048,128]{1,0:T(8,128)(2,1)} %param.23, f32[1024,1,128]{2,0,1:T(8,128)S(1)} %get-tuple-element.172, f32[128]{0:T(128)S(1)} %copy-done.16, f32[1024]{0:T(1024)S(1)} %add_rsqrt_fusion.1), kind=kOutput, calls=%fused_computation.85 | convolution fusion | flops 538181632 | bytes 5509632 | tf_op jit(solution)/shard_map/dot_general | solution.py:117
  158.4 1.3 multiply_reduce_fusion
  160.3 62.6 %all_to_all.21 = bf16[8,1024,256]{2,1,0:T(8,128)(2,1)S(1)} all-to-all(bf16[8,1024,256]{2,1,0:T(8,128)(2,1)S(1)} %stack.2), channel_id=1, replica_groups=mesh['sp_0'=8,'sp_1'=4,'tp'=8] {'tp'}, dimensions={0} | all-to-all | bytes 8388608 | tf_op jit(solution)/shard_map/all_to_all | solution.py:177
  222.9 2.1 fusion.38
  (241 shorter events, 45.6 us)
Async XLA Ops:
  0.0 24.3 %copy-start = (bf16[2048,128]{1,0:T(8,128)(2,1)S(1)}, bf16[2048,128]{1,0:T(8,128)(2,1)}, u32[]{:S(2)}) copy-start(bf16[2048,128]{1,0:T(8,128)(2,1)} %param.21) | copy-start | bytes 1572868
  0.0 3.5 %copy-start.4 = (bf16[1024,2048]{1,0:T(8,128)(2,1)S(1)}, bf16[1024,2048]{1,0:T(8,128)(2,1)}, u32[]{:S(2)}) copy-start(bf16[1024,2048]{1,0:T(8,128)(2,1)} %param.18) | copy-start | bytes 12582916
  0.0 3.5 %copy-start.9 = (f32[2048]{0:T(1024)S(1)}, f32[2048]{0:T(1024)}, u32[]{:S(2)}) copy-start(f32[2048]{0:T(1024)} %param.19) | copy-start | bytes 24580
  3.5 1.0 copy-start.5
  4.6 2.7 %copy-start.1 = (bf16[1024,2048]{1,0:T(8,128)(2,1)}, bf16[1024,2048]{1,0:T(8,128)(2,1)S(1)}, u32[]{:S(2)}) copy-start(bf16[1024,2048]{1,0:T(8,128)(2,1)S(1)} %fusion.32) | copy-start | bytes 12582916
  4.6 1.4 copy-start.6
  6.0 5.3 %copy-start.7 = (bf16[128,2048]{1,0:T(8,128)(2,1)S(1)}, bf16[128,2048]{1,0:T(8,128)(2,1)}, u32[]{:S(2)}) copy-start(bf16[128,2048]{1,0:T(8,128)(2,1)} %param.32) | copy-start | bytes 1572868
  6.0 5.6 %copy-start.8 = (bf16[128,2048]{1,0:T(8,128)(2,1)S(1)}, bf16[128,2048]{1,0:T(8,128)(2,1)}, u32[]{:S(2)}) copy-start(bf16[128,2048]{1,0:T(8,128)(2,1)} %param.33) | copy-start | bytes 1572868
  7.2 11.3 %copy-start.11 = (f32[128]{0:T(128)S(1)}, f32[128]{0:T(128)}, u32[]{:S(2)}) copy-start(f32[128]{0:T(128)} %param.27) | copy-start | bytes 1540
  7.3 151.0 %collective-permute-start = (bf16[2,128]{1,0:T(2,128)(2,1)S(1)}, bf16[2,128]{1,0:T(2,128)(2,1)S(1)}, u32[]{:S(2)}, u32[]{:S(2)}) collective-permute-start(bf16[2,128]{1,0:T(2,128)(2,1)S(1)} %slice.193), channel_id=1, source_target_pairs={{0,8},{8,16},{16,24},{24,32},{32,40},{40,48},{48,56},{56,64},{64,7... | collective-permute-start | bytes 1544 | tf_op jit(solution)/shard_map/ppermute | solution.py:17
  13.3 146.7 %all-to-all-start.1 = ((bf16[256,8,256]{2,0,1:T(8,128)(2,1)}), bf16[256,8,256]{2,0,1:T(8,128)(2,1)S(1)}, u32[]{:S(2)}, u32[]{:S(2)}) async-start(bf16[256,8,256]{2,0,1:T(8,128)(2,1)} %copy.57), calls=%async_computation.1 | async-start | bytes 2097152 | tf_op jit(solution)/shard_map/all_to_all | solution.py:175
  18.6 3.7 %copy-start.2 = (bf16[1024,2048]{1,0:T(8,128)(2,1)S(1)}, bf16[1024,2048]{1,0:T(8,128)(2,1)}, u32[]{:S(2)}) copy-start(bf16[1024,2048]{1,0:T(8,128)(2,1)} %copy-done.1) | copy-start | bytes 12582916
  18.6 3.7 %copy-start.13 = (bf16[2048,128]{1,0:T(8,128)(2,1)S(1)}, bf16[2048,128]{1,0:T(8,128)(2,1)}, u32[]{:S(2)}) copy-start(bf16[2048,128]{1,0:T(8,128)(2,1)} %param.22) | copy-start | bytes 1572868
  22.3 2.0 copy-start.14
  120.6 33.9 %copy-start.10 = (bf16[3,128]{1,0:T(4,128)(2,1)S(1)}, bf16[3,128]{1,0:T(4,128)(2,1)}, u32[]{:S(2)}) copy-start(bf16[3,128]{1,0:T(4,128)(2,1)} %param.30) | copy-start | bytes 2308
  120.6 33.9 %copy-start.16 = (f32[128]{0:T(128)S(1)}, f32[128]{0:T(128)}, u32[]{:S(2)}) copy-start(f32[128]{0:T(128)} %param.29) | copy-start | bytes 1540
  154.5 3.8 %copy-start.3 = (bf16[1024,2048]{1,0:T(8,128)(2,1)S(1)}, bf16[1024,2048]{1,0:T(8,128)(2,1)}, u32[]{:S(2)}) copy-start(bf16[1024,2048]{1,0:T(8,128)(2,1)} %copy-done.1) | copy-start | bytes 12582916
  154.5 3.8 %copy-start.15 = (bf16[2048,128]{1,0:T(8,128)(2,1)S(1)}, bf16[2048,128]{1,0:T(8,128)(2,1)}, u32[]{:S(2)}) copy-start(bf16[2048,128]{1,0:T(8,128)(2,1)} %param.25) | copy-start | bytes 1572868
  158.4 1.4 copy-start.12
